TPU v7x, 32 devices: a whole 2x2x4 slice. The times are simulated.
32 devices in a mesh: rep: 2 (over x), fs: 8 (over z, y), tp: 2 (over core).
Axes of the slice: x: 2, y: 2, z: 4, core: 2. Of those that a mesh axis runs over, the one named last changes fastest.
Arguments:
- tokens: bfloat16 [12288, 2048], P(('rep', 'fs', 'tp')), may hold values from -6 to 6
- outer_weight: float32 [2048, 1536], P('fs', 'tp'), may hold values from -0.125 to 0.125
- inner_weight: float32 [2048, 1536], P('fs', 'tp'), may hold values from -0.125 to 0.125
- value_weight: float32 [2048, 1536], P('fs', 'tp'), may hold values from -0.125 to 0.125
- conv_taps: float32 [3, 1536], P(None, 'tp'), may hold values from -3 to 3
- mix_out: float32 [1536, 2048], P('tp', 'fs'), may hold values from -0.15625 to 0.15625
- norm_first: float32 [2048], replicated, may hold values from 0.1 to 1.9
- up_weight: float32 [2048, 4096], P('fs', 'tp'), may hold values from -0.125 to 0.125
- down_weight: float32 [4096, 2048], P('tp', 'fs'), may hold values from -0.09375 to 0.09375
- norm_second: float32 [2048], replicated, may hold values from 0.1 to 1.9
Outputs:
- encoded: bfloat16 [12288, 2048], P(('rep', 'fs', 'tp'))
All inputs are finite; a program needn't handle non-finite values.
Results may differ from a plain program's by a relative error of at most 0.015.
Values may be sent and summed in bfloat16 or wider, within the bound.
A program may use at most 128 MiB of HBM per device.

v0:
```python
import jax
import jax.numpy as jnp
from jax import lax
from jax.sharding import PartitionSpec as P

SEQ = 128


residual_scale = 2.0**0.25
norm_epsilon = 1e-05


def layer_norm(values, scaling):
    center = values - jnp.mean(values, axis=-1, keepdims=True)
    spread = jnp.mean(center * center, axis=-1, keepdims=True)
    return center * lax.rsqrt(spread + norm_epsilon) * scaling


def short_conv(product, conv_taps):
    places = jnp.arange(product.shape[0], dtype=jnp.int32) % SEQ
    blank = jnp.zeros((1, product.shape[1]), jnp.float32)
    before = jnp.concatenate([blank, product[:-1]], axis=0)
    after = jnp.concatenate([product[1:], blank], axis=0)
    before = jnp.where((places > 0)[:, None], before, 0.0)
    after = jnp.where((places < SEQ - 1)[:, None], after, 0.0)
    return conv_taps[0] * before + conv_taps[1] * product + conv_taps[2] * after


def local(
    tokens,
    outer_weight,
    inner_weight,
    value_weight,
    conv_taps,
    mix_out,
    norm_first,
    up_weight,
    down_weight,
    norm_second,
):
    grouped = lax.all_gather(tokens, "tp", axis=0, tiled=True)
    outer_bf = outer_weight.astype(jnp.bfloat16)
    inner_bf = inner_weight.astype(jnp.bfloat16)
    value_bf = value_weight.astype(jnp.bfloat16)
    outer_full, inner_full, value_full = (
        lax.all_gather(outer_bf, "fs", axis=0, tiled=True),
        lax.all_gather(inner_bf, "fs", axis=0, tiled=True),
        lax.all_gather(value_bf, "fs", axis=0, tiled=True),
    )
    outer = jnp.dot(grouped, outer_full, preferred_element_type=jnp.float32)
    inner = jnp.dot(grouped, inner_full, preferred_element_type=jnp.float32)
    value = jnp.dot(grouped, value_full, preferred_element_type=jnp.float32)
    mixed = (outer * short_conv(inner * value, conv_taps)).astype(jnp.bfloat16)
    mixout_full = lax.all_gather(mix_out.astype(jnp.bfloat16), "fs", axis=1, tiled=True)
    selected = mixed
    mixing = lax.psum_scatter(
        jnp.dot(selected, mixout_full, preferred_element_type=jnp.float32).astype(jnp.bfloat16),
        "tp",
        scatter_dimension=0,
        tiled=True,
    ).astype(jnp.float32)
    first = layer_norm(residual_scale * tokens.astype(jnp.float32) + mixing, norm_first).astype(
        jnp.bfloat16
    )
    grouped_first = lax.all_gather(first, "tp", axis=0, tiled=True)
    upward_bf = up_weight.astype(jnp.bfloat16)
    upward_full = lax.all_gather(upward_bf, "fs", axis=0, tiled=True)
    raised = jnp.dot(grouped_first, upward_full, preferred_element_type=jnp.float32)
    raised = jax.nn.relu(raised)
    hidden = (raised * raised).astype(jnp.bfloat16)
    down_full = lax.all_gather(down_weight.astype(jnp.bfloat16), "fs", axis=1, tiled=True)
    selected = hidden
    lowered = lax.psum_scatter(
        jnp.dot(selected, down_full, preferred_element_type=jnp.float32).astype(jnp.bfloat16),
        "tp",
        scatter_dimension=0,
        tiled=True,
    ).astype(jnp.float32)
    return layer_norm(residual_scale * first.astype(jnp.float32) + lowered, norm_second).astype(
        jnp.bfloat16
    )


def solution(mesh):
    return jax.shard_map(
        local,
        mesh=mesh,
        in_specs=(
            P(("rep", "fs", "tp"), None),
            P("fs", "tp"),
            P("fs", "tp"),
            P("fs", "tp"),
            P(None, "tp"),
            P("tp", "fs"),
            P(),
            P("fs", "tp"),
            P("tp", "fs"),
            P(),
        ),
        out_specs=P(("rep", "fs", "tp"), None),
        check_vma=False,
    )
```

profile of v0, /device:TPU:0, one launch (start us, length us, event | category | flops | bytes accessed | tf_op | source)
XLA Modules:
  0.0 593.9 jit_solution(13553452324385656310)
XLA Ops:
  7.3 1.9 convert_element_type.50
  9.3 0.8 convert_element_type.51
  12.0 11.7 %all-gather.9.cloned.1.call-done = bf16[768,2048]{1,0:T(8,128)(2,1)} async-done(((bf16[384,2048]{1,0:T(8,128)(2,1)}), bf16[768,2048]{1,0:T(8,128)(2,1)}) %all-gather.9.cloned.1.call-update) | async-done | bytes 3145744 | tf_op jit(solution)/shard_map/all_gather | solution.py:41
  23.8 63.4 %all-gather.13.cloned.1.call-done = bf16[2048,768]{1,0:T(8,128)(2,1)} async-done(((bf16[256,768]{1,0:T(8,128)(2,1)}), bf16[2048,768]{1,0:T(8,128)(2,1)}) %all-gather.13.cloned.1.call-update) | async-done | bytes 3145744 | tf_op jit(solution)/shard_map/all_gather | solution.py:47
  87.2 6.8 %fusion.9 = f32[768,768]{1,0:T(8,128)} fusion(bf16[768,2048]{1,0:T(8,128)(2,1)} %all-gather.9.cloned.1.call-done, bf16[2048,768]{1,0:T(8,128)(2,1)} %all-gather.13.cloned.1.call-done), kind=kOutput, calls=%fused_computation.29 | convolution fusion | flops 2415919104 | bytes 8650752 | tf_op jit(solution)/shard_map/dot_general | solution.py:51
  94.0 54.1 %all-gather.15.cloned.1.call-done = bf16[2048,768]{1,0:T(8,128)(2,1)} async-done(((bf16[256,768]{1,0:T(8,128)(2,1)}), bf16[2048,768]{1,0:T(8,128)(2,1)}) %all-gather.15.cloned.1.call-update) | async-done | bytes 3145744 | tf_op jit(solution)/shard_map/all_gather | solution.py:48
  148.1 6.1 %convolution_multiply_fusion = f32[768,768]{1,0:T(8,128)S(1)} fusion(f32[768,768]{1,0:T(8,128)} %fusion.9, bf16[768,2048]{1,0:T(8,128)(2,1)} %all-gather.9.cloned.1.call-done, bf16[2048,768]{1,0:T(8,128)(2,1)} %all-gather.15.cloned.1.call-done), kind=kOutput, calls=%fused_computation.12 | convolution fusion | flops 2416508928 | bytes 11010048 | tf_op jit(solution)/shard_map/dot_general | solution.py:52
  154.2 2.5 fusion.8
  156.7 52.1 %all-gather.11.cloned.1.call-done = bf16[2048,768]{1,0:T(8,128)(2,1)} async-done(((bf16[256,768]{1,0:T(8,128)(2,1)}), bf16[2048,768]{1,0:T(8,128)(2,1)}) %all-gather.11.cloned.1.call-update) | async-done | bytes 3145744 | tf_op jit(solution)/shard_map/all_gather | solution.py:46
  208.8 63.2 %all-gather.17.cloned.1.call-done = bf16[768,2048]{1,0:T(8,128)(2,1)} async-done(((bf16[768,256]{1,0:T(8,128)(2,1)}), bf16[768,2048]{1,0:T(8,128)(2,1)}) %all-gather.17.cloned.1.call-update) | async-done | bytes 3145744 | tf_op jit(solution)/shard_map/all_gather | solution.py:54
  272.1 12.8 %convolution_convert_fusion.1 = bf16[768,2048]{1,0:T(8,128)(2,1)} fusion(bf16[768,2048]{1,0:T(8,128)(2,1)} %all-gather.17.cloned.1.call-done, f32[767,768]{1,0:T(8,128)} %get-tuple-element.9, f32[768,768]{1,0:T(8,128)S(1)} %convolution_multiply_fusion, f32[767,768]{1,0:T(8,128)} %get-tuple-element.8, bf16[768,2048]{1,0:T(8,128)(2,1)} %all-gather.9.cloned.1.call-done, ...), kind=kOutput, calls=%fused_computation.2 | convolution fusion | flops 4838719488 | bytes 19665408 | tf_op jit(solution)/shard_map/dot_general | solution.py:57
  285.0 2.9 convert_element_type.58
  288.1 6.3 %reduce-scatter.3.cloned.1.call-done = bf16[384,2048]{1,0:T(8,128)(2,1)} async-done(((bf16[768,2048]{1,0:T(8,128)(2,1)}), bf16[384,2048]{1,0:T(8,128)(2,1)}) %reduce-scatter.3.cloned.1.call-update) | async-done | bytes 1572880 | tf_op jit(solution)/shard_map/reduce_scatter | solution.py:56
  294.4 2.1 fusion
  297.4 2.0 multiply_convert_fusion.2
  299.4 2.7 convert_element_type.60
  302.2 120.2 %all-gather.21.cloned.1.call-done = bf16[2048,2048]{1,0:T(8,128)(2,1)} async-done(((bf16[256,2048]{1,0:T(8,128)(2,1)}), bf16[2048,2048]{1,0:T(8,128)(2,1)}) %all-gather.21.cloned.1.call-update) | async-done | bytes 8388624 | tf_op jit(solution)/shard_map/all_gather | solution.py:67
  422.3 11.9 %all-gather.19.cloned.1.call-done = bf16[768,2048]{1,0:T(8,128)(2,1)} async-done(((bf16[384,2048]{1,0:T(8,128)(2,1)}), bf16[768,2048]{1,0:T(8,128)(2,1)}) %all-gather.19.cloned.1.call-update) | async-done | bytes 3145744 | tf_op jit(solution)/shard_map/all_gather | solution.py:65
  434.2 10.0 %multiply_convert_fusion = bf16[768,2048]{1,0:T(8,128)(2,1)S(1)} fusion(bf16[768,2048]{1,0:T(8,128)(2,1)} %all-gather.19.cloned.1.call-done, bf16[2048,2048]{1,0:T(8,128)(2,1)} %all-gather.21.cloned.1.call-done), kind=kOutput, calls=%fused_computation | convolution fusion | flops 6447169536 | bytes 14680064 | tf_op jit(solution)/shard_map/dot_general | solution.py:68
  444.3 118.2 %all-gather.23.cloned.1.call-done = bf16[2048,2048]{1,0:T(8,128)(2,1)} async-done(((bf16[2048,256]{1,0:T(8,128)(2,1)}), bf16[2048,2048]{1,0:T(8,128)(2,1)}) %all-gather.23.cloned.1.call-update) | async-done | bytes 8388624 | tf_op jit(solution)/shard_map/all_gather | solution.py:71
  562.4 10.2 %convolution_convert_fusion = bf16[768,2048]{1,0:T(8,128)(2,1)} fusion(bf16[768,2048]{1,0:T(8,128)(2,1)S(1)} %multiply_convert_fusion, bf16[2048,2048]{1,0:T(8,128)(2,1)} %all-gather.23.cloned.1.call-done), kind=kOutput, calls=%fused_computation.1 | convolution fusion | flops 6444023808 | bytes 14680064 | tf_op jit(solution)/shard_map/dot_general | solution.py:74
  572.7 9.5 %reduce-scatter.5.cloned.1.call-done = bf16[384,2048]{1,0:T(8,128)(2,1)} async-done(((bf16[768,2048]{1,0:T(8,128)(2,1)}), bf16[384,2048]{1,0:T(8,128)(2,1)}) %reduce-scatter.5.cloned.1.call-update) | async-done | bytes 1572880 | tf_op jit(solution)/shard_map/reduce_scatter | solution.py:73
  582.2 2.1 fusion.1
  585.1 2.0 multiply_convert_fusion.1
  (50 shorter events, 4.7 us)
Async XLA Ops:
  6.5 2.8 copy-start.4
  6.5 3.7 copy-start.5
  6.5 4.5 copy-start.6
  6.5 17.2 %all-gather.9.cloned.1.call-start = ((), (), s32[]{:S(2)}) async-start(), calls=%async_computation.2 | async-start | bytes 4718592 | tf_op jit(solution)/shard_map/all_gather | solution.py:41
  7.3 4.7 copy-start.9
  7.3 79.9 %all-gather.13.cloned.1.call-start = ((), (), s32[]{:S(2)}) async-start(), calls=%async_computation.4 | async-start | bytes 3538944 | tf_op jit(solution)/shard_map/all_gather | solution.py:47
  9.3 138.8 %all-gather.15.cloned.1.call-start = ((), (), s32[]{:S(2)}) async-start(), calls=%async_computation.5 | async-start | bytes 3538944 | tf_op jit(solution)/shard_map/all_gather | solution.py:48
  10.2 198.7 %all-gather.11.cloned.1.call-start = ((), (), s32[]{:S(2)}) async-start(), calls=%async_computation.3 | async-start | bytes 3538944 | tf_op jit(solution)/shard_map/all_gather | solution.py:46
  11.0 261.0 %all-gather.17.cloned.1.call-start = ((), (), s32[]{:S(2)}) async-start(), calls=%async_computation.6 | async-start | bytes 3538944 | tf_op jit(solution)/shard_map/all_gather | solution.py:54
  11.9 282.5 %reduce-scatter.3.cloned.1.call-start = ((), (), s32[]{:S(2)}) async-start(), calls=%async_computation.7 | async-start | bytes 4718592 | tf_op jit(solution)/shard_map/reduce_scatter | solution.py:56
  284.9 9.5 %copy-start.1 = (bf16[384,2048]{1,0:T(8,128)(2,1)S(1)}, bf16[384,2048]{1,0:T(8,128)(2,1)}, u32[]{:S(2)}) copy-start(bf16[384,2048]{1,0:T(8,128)(2,1)} %param.10) | copy-start | bytes 4718596
  284.9 137.4 %all-gather.21.cloned.1.call-start = ((), (), s32[]{:S(2)}) async-start(), calls=%async_computation.9 | async-start | bytes 9437184 | tf_op jit(solution)/shard_map/all_gather | solution.py:67
  287.9 9.5 %copy-start.7 = (f32[2048]{0:T(1024)S(1)}, f32[2048]{0:T(1024)}, u32[]{:S(2)}) copy-start(f32[2048]{0:T(1024)} %param.16) | copy-start | bytes 24580
  287.9 146.3 %all-gather.19.cloned.1.call-start = ((), (), s32[]{:S(2)}) async-start(), calls=%async_computation.8 | async-start | bytes 4718592 | tf_op jit(solution)/shard_map/all_gather | solution.py:65
  294.4 2.1 copy-start.2
  299.4 263.0 %all-gather.23.cloned.1.call-start = ((), (), s32[]{:S(2)}) async-start(), calls=%async_computation.10 | async-start | bytes 9437184 | tf_op jit(solution)/shard_map/all_gather | solution.py:71
  302.1 280.0 %reduce-scatter.5.cloned.1.call-start = ((), (), s32[]{:S(2)}) async-start(), calls=%async_computation.11 | async-start | bytes 4718592 | tf_op jit(solution)/shard_map/reduce_scatter | solution.py:73
  572.6 9.5 %copy-start = (bf16[384,2048]{1,0:T(8,128)(2,1)S(1)}, bf16[384,2048]{1,0:T(8,128)(2,1)}, u32[]{:S(2)}) copy-start(bf16[384,2048]{1,0:T(8,128)(2,1)} %multiply_convert_fusion.2) | copy-start | bytes 4718596
  572.7 12.5 %copy-start.8 = (f32[2048]{0:T(1024)S(1)}, f32[2048]{0:T(1024)}, u32[]{:S(2)}) copy-start(f32[2048]{0:T(1024)} %param.19) | copy-start | bytes 24580
  582.2 2.1 copy-start.3
Sparse Core Ops, SparseCore 0:
  8.9 14.8 all-gather.8
  25.9 61.1 all-gather.12
  89.4 58.6 all-gather.14
  150.1 58.6 all-gather.10
  210.7 61.3 all-gather.16
  285.0 9.3 reduce-scatter.2
  296.6 125.7 all-gather.20
  423.9 10.2 all-gather.18
  436.3 126.0 all-gather.22
  572.8 9.3 reduce-scatter.4
where the time goes:
time: 594 us
  waiting for transfers between devices  511 us (86%)
  matrix products  46.1 us (8%)
  other arithmetic  19.7 us (3%)
  between operations  13.6 us (2%)
    all_gather x1, waiting for transfers between devices, local(): upward_full = lax.all_gather(upward_bf, 'fs', axis=0, tiled=True)  120 us
    all_gather x1, waiting for transfers between devices, local(): lax.all_gather(down_weight.astype(jnp.bfloat16), 'fs', axis=1, tiled=True)  118 us
    all_gather x1, waiting for transfers between devices, local(): lax.all_gather(inner_bf, 'fs', axis=0, tiled=True)  63.4 us
    all_gather x1, waiting for transfers between devices, local(): lax.all_gather(mix_out.astype(jnp.bfloat16), 'fs', axis=1, tiled=True)  63.2 us
    all_gather x1, waiting for transfers between devices, local(): lax.all_gather(value_bf, 'fs', axis=0, tiled=True)  54.1 us
    all_gather x1, waiting for transfers between devices, local(): lax.all_gather(outer_bf, 'fs', axis=0, tiled=True)  52.1 us
    dot_general x1, matrix products, local(): jnp.dot(selected, mixout_full, preferred_element_type=jnp.float32)  12.8 us
  transfers between devices with their start and end apart: 10, of which 10 were waited for; matrix products, arithmetic and copies ran while one was open for 7% of the time, Pallas kernels for 0%

commit v1 on v0

--- a/solution.py
+++ b/solution.py
@@ -1,6 +1,10 @@
+import functools
+
 import jax
 import jax.numpy as jnp
 from jax import lax
+from jax.experimental import pallas as pl
+from jax.experimental.pallas import tpu as pltpu
 from jax.sharding import PartitionSpec as P
 
 SEQ = 128
@@ -81,9 +85,529 @@
     )
 
 
+MESH = pl.DeviceIdType.MESH
+BF = jnp.bfloat16
+F32 = jnp.float32
+
+
+def dot(a, b):
+    return jnp.dot(a, b, preferred_element_type=F32)
+
+
+def third_rows(rows):
+    return (rows // 3 + 8) // 16 * 16
+
+
+def layer_kernel(
+    n,
+    tokens_hbm,
+    outer_hbm,
+    inner_hbm,
+    value_hbm,
+    taps_ref,
+    mix_hbm,
+    norm1_ref,
+    up_hbm,
+    down_hbm,
+    norm2_ref,
+    out_ref,
+    wa,
+    wb,
+    wc,
+    wd,
+    stage_a,
+    stage_b,
+    stage_d,
+    tok,
+    acc,
+    mixed,
+    own,
+    psend,
+    precv1,
+    precv2,
+    fst,
+    hid,
+    load_sem,
+    ring_send,
+    ring_recv,
+    tp_send,
+    tp_recv,
+):
+    half = n // 2
+    r = lax.axis_index("rep")
+    f = lax.axis_index("fs")
+    t = lax.axis_index("tp")
+    rows = tokens_hbm.shape[0]
+    both = 2 * rows
+    d = tokens_hbm.shape[1]
+    ks = wa.shape[2]
+    wch = wa.shape[3]
+    ff = wc.shape[2]
+    nc = wb.shape[2]
+
+    odd = f % 2
+    pos = (1 - odd) * (f // 2) + odd * (n - 1 - f // 2)
+
+    def at(place):
+        p = (place + 2 * n) % n
+        hi = p // half
+        return (1 - hi) * (2 * p) + hi * (2 * (n - 1 - p) + 1)
+
+    right = {"fs": at(pos + 1)}
+    left = {"fs": at(pos - 1)}
+    across = {"rep": 1 - r}
+    mate = {"tp": 1 - t}
+
+    loads = [
+        pltpu.make_async_copy(outer_hbm, stage_a.at[0], load_sem.at[0]),
+        pltpu.make_async_copy(inner_hbm, stage_a.at[1], load_sem.at[1]),
+        pltpu.make_async_copy(value_hbm, stage_a.at[2], load_sem.at[2]),
+        pltpu.make_async_copy(mix_hbm, stage_b, load_sem.at[3]),
+        pltpu.make_async_copy(
+            up_hbm, acc.at[pl.ds(0, ks), pl.ds(0, ff)], load_sem.at[4]
+        ),
+        pltpu.make_async_copy(down_hbm, stage_d, load_sem.at[5]),
+        pltpu.make_async_copy(tokens_hbm, tok.at[pl.ds(0, rows)], load_sem.at[6]),
+    ]
+    for load in loads:
+        load.start()
+
+    barrier = pltpu.get_barrier_semaphore()
+    for device in (right, left, across, mate):
+        pl.semaphore_signal(barrier, inc=1, device_id=device, device_id_type=MESH)
+    pl.semaphore_wait(barrier, 4)
+
+    def mate_copy(i, src, dst):
+        return pltpu.make_async_remote_copy(
+            src_ref=src,
+            dst_ref=dst,
+            send_sem=tp_send.at[i],
+            recv_sem=tp_recv.at[i],
+            device_id=mate,
+            device_id_type=MESH,
+        )
+
+    def piece(ti, which, owner):
+        if ti == 0:
+            return wa.at[2 if which else r, owner]
+        ref = (None, wb, wc, wd)[ti]
+        u = third_rows(ref.shape[1])
+        if which:
+            return ref.at[owner, pl.ds(2 * u, ref.shape[1] - 2 * u)]
+        return ref.at[owner, pl.ds(pl.multiple_of(r * u, 16), u)]
+
+    per = 6 * half - 3
+    index = {}
+    for h in range(1, half + 1):
+        for kind in ("Rq", "Rp", "Lq", "Lp", "XR", "XL"):
+            if h == half and kind in ("Rp", "Lq", "XL"):
+                continue
+            index[kind, h] = len(index)
+
+    copies = {}
+
+    def message(ti, kind, h):
+        key = (ti, kind, h)
+        if key not in copies:
+            which = kind[1] == "p"
+            if kind[0] == "R":
+                src, device = at(pos - (h - 1)), right
+            elif kind[0] == "L":
+                src, device = at(pos + (h - 1)), left
+            else:
+                src, device = at(pos - h if kind == "XR" else pos + h), across
+            i = ti * per + index[kind, h]
+            ref = piece(ti, which, src)
+            copies[key] = pltpu.make_async_remote_copy(
+                src_ref=ref,
+                dst_ref=ref,
+                send_sem=ring_send.at[i],
+                recv_sem=ring_recv.at[i],
+                device_id=device,
+                device_id_type=MESH,
+            )
+        return copies[key]
+
+    def send(ti, kind, h):
+        if ti < 4 and (kind, h) in index:
+            message(ti, kind, h).start()
+
+    def got(ti, kind, h):
+        message(ti, kind, h).wait_recv()
+
+    def event(ti, h, which):
+        if which == 0:
+            got(ti, "Rq", h)
+            send(ti, "Rq", h + 1)
+            send(ti, "XR", h)
+            if h < half:
+                got(ti, "Lq", h)
+                if h + 1 < half:
+                    send(ti, "Lq", h + 1)
+                else:
+                    send(ti + 1, "Lq", 1)
+                send(ti, "XL", h)
+            else:
+                send(ti + 1, "Rp", 1)
+                got(ti, "Lp", h)
+                send(ti + 1, "Lp", 1)
+        else:
+            got(ti, "Rp", h)
+            if h + 1 < half:
+                send(ti, "Rp", h + 1)
+            else:
+                send(ti + 1, "Rq", 1)
+            got(ti, "Lp", h)
+            send(ti, "Lp", h + 1)
+
+    def events(ti):
+        out = []
+        for h in range(1, half + 1):
+            out.append((ti, h, 0))
+            if h < half:
+                out.append((ti, h, 1))
+        return out
+
+    def arrived(ti, h):
+        got(ti, "XR", h)
+        if h < half:
+            got(ti, "XL", h)
+
+    def owners(h):
+        if h == 0:
+            return [f]
+        if h == half:
+            return [at(pos + half)]
+        return [at(pos - h), at(pos + h)]
+
+    for i in range(3):
+        loads[i].wait()
+        wa[i, f] = stage_a[i].astype(BF)
+    send(0, "Rq", 1)
+    send(0, "Lq", 1)
+    send(0, "Rp", 1)
+    send(0, "Lp", 1)
+    share = mate_copy(0, tokens_hbm, tok.at[pl.ds(rows, rows)])
+    share.start()
+    loads[3].wait()
+    wb[f] = stage_b[...].astype(BF)
+    loads[4].wait()
+    wc[f] = acc[pl.ds(0, ks), pl.ds(0, ff)].astype(BF)
+    loads[5].wait()
+    wd[f] = stage_d[...].astype(BF)
+    loads[6].wait()
+    share.wait_recv()
+
+    tn = 256
+
+    def accumulate(x_ref, h, weight, width, base):
+        who = owners(h)
+
+        def unit(i, _):
+            m = pl.multiple_of((i % 2) * rows, 16)
+            c = pl.multiple_of((i // 2) * tn, tn)
+            total = None
+            for o in who:
+                x = x_ref[pl.ds(m, rows), pl.ds(pl.multiple_of(o * ks, 128), ks)]
+                term = dot(x, weight(o, pl.ds(c, tn)))
+                total = term if total is None else total + term
+            span = pl.ds(pl.multiple_of(base + c, tn), tn)
+            if h == 0:
+                acc[pl.ds(m, rows), span] = total
+            else:
+                acc[pl.ds(m, rows), span] += total
+            return 0
+
+        lax.fori_loop(0, 2 * (width // tn), unit, 0)
+
+    def project(h):
+        for i in range(3):
+            accumulate(tok, h, lambda o, c, i=i: wa[i, o, :, c], wch, i * wch)
+
+    def raise_(h):
+        accumulate(fst, h, lambda o, c: wc[o, :, c], ff, 0)
+
+    def lower(x_ref, w_ref, h, recv, first_sem):
+        for k, o in enumerate(owners(h)):
+            psend[o] = dot(x_ref[pl.ds(rows, rows), :], w_ref[o]).astype(BF)
+            mate_block(first_sem, h, k, o, recv).start()
+            own[o] = dot(x_ref[pl.ds(0, rows), :], w_ref[o])
+
+    def mate_block(first_sem, h, k, o, recv):
+        i = first_sem + (0 if h == 0 else 2 * h - 1 + k)
+        return mate_copy(i, psend.at[o], recv.at[o])
+
+    def mate_blocks(first_sem, recv):
+        return [
+            mate_block(first_sem, h, k, o, recv)
+            for h in range(half + 1)
+            for k, o in enumerate(owners(h))
+        ]
+
+    def mix():
+        seq = SEQ
+
+        def unit(i, _):
+            m = pl.multiple_of((i % (both // seq)) * seq, seq)
+            c = pl.multiple_of((i // (both // seq)) * tn, tn)
+            o = acc[pl.ds(m, seq), pl.ds(c, tn)]
+            p = (
+                acc[pl.ds(m, seq), pl.ds(pl.multiple_of(wch + c, tn), tn)]
+                * acc[pl.ds(m, seq), pl.ds(pl.multiple_of(2 * wch + c, tn), tn)]
+            )
+            place = lax.broadcasted_iota(jnp.int32, p.shape, 0)
+            before = jnp.where(place > 0, pltpu.roll(p, 1, 0), 0.0)
+            after = jnp.where(place < seq - 1, pltpu.roll(p, seq - 1, 0), 0.0)
+            taps = taps_ref[:, pl.ds(c, tn)]
+            conv = taps[0:1] * before + taps[1:2] * p + taps[2:3] * after
+            mixed[pl.ds(m, seq), pl.ds(c, tn)] = (o * conv).astype(BF)
+            return 0
+
+        lax.fori_loop(0, (both // seq) * (wch // tn), unit, 0)
+
+    def norm(base_ref, recv, gain_ref, dest_ref):
+        tm = 32
+
+        def unit(i, _):
+            m = pl.multiple_of(i * tm, tm)
+            parts = [
+                residual_scale
+                * base_ref[pl.ds(m, tm), pl.ds(b * nc, nc)].astype(F32)
+                + own[b, pl.ds(m, tm)]
+                + recv[b, pl.ds(m, tm)].astype(F32)
+                for b in range(n)
+            ]
+            total = parts[0]
+            for b in range(1, n):
+                total = total + parts[b]
+            mean = jnp.sum(total, axis=-1, keepdims=True) / d
+            parts = [p - mean for p in parts]
+            square = parts[0] * parts[0]
+            for b in range(1, n):
+                square = square + parts[b] * parts[b]
+            spread = jnp.sum(square, axis=-1, keepdims=True) / d
+            scale = lax.rsqrt(spread + norm_epsilon)
+            for b in range(n):
+                cols = pl.ds(b * nc, nc)
+                dest_ref[pl.ds(m, tm), cols] = (
+                    parts[b] * scale * gain_ref[:, cols]
+                ).astype(BF)
+            return 0
+
+        lax.fori_loop(0, rows // tm, unit, 0)
+
+    def square_relu():
+        def unit(i, _):
+            m = pl.multiple_of((i % (both // 128)) * 128, 128)
+            c = pl.multiple_of((i // (both // 128)) * tn, tn)
+            v = jnp.maximum(acc[pl.ds(m, 128), pl.ds(c, tn)], 0.0)
+            hid[pl.ds(m, 128), pl.ds(c, tn)] = (v * v).astype(BF)
+            return 0
+
+        lax.fori_loop(0, (both // 128) * (ff // tn), unit, 0)
+
+    mix_sem, first_sem, low_sem = 1, 1 + n, 2 + n
+    give = mate_copy(first_sem, fst.at[pl.ds(0, rows)], fst.at[pl.ds(rows, rows)])
+
+    plan = {}
+
+    def after(ti, h, which, work):
+        plan.setdefault((ti, h, which), []).append(work)
+
+    def project_at(h):
+        def work():
+            if h:
+                arrived(0, h)
+            project(h)
+
+        return work
+
+    def mixout_at(h):
+        def work():
+            if h:
+                arrived(1, h)
+            lower(mixed, wb, h, precv1, mix_sem)
+
+        return work
+
+    def raise_at(h):
+        def work():
+            if h:
+                arrived(2, h)
+            raise_(h)
+
+        return work
+
+    def lower_at(h):
+        def work():
+            if h:
+                arrived(3, h)
+            lower(hid, wd, h, precv2, low_sem)
+
+        return work
+
+    def first_half():
+        for c in mate_blocks(mix_sem, precv1):
+            c.wait_recv()
+        norm(tok, precv1, norm1_ref, fst)
+        give.start()
+
+    def start_raise():
+        give.wait_recv()
+        raise_(0)
+
+    after(0, 1, 0, lambda: project(0))
+    for h in range(1, half - 1):
+        after(0, h + 1, 1, project_at(h))
+    after(1, 1, 0, project_at(half - 1))
+    after(1, 1, 1, project_at(half))
+    after(1, 2, 0, mix)
+    after(1, half - 1, 0, mixout_at(0))
+    for h in range(1, half - 1):
+        after(1, half - 1 if h < half - 2 else half, 0, mixout_at(h))
+    after(2, 1, 0, mixout_at(half - 1))
+    after(2, 1, 0, mixout_at(half))
+    after(2, 1, 1, first_half)
+    after(2, 2, 0, start_raise)
+    for h in range(1, half - 1):
+        after(2, h + 1, 1, raise_at(h))
+    after(3, 1, 0, raise_at(half - 1))
+    after(3, 1, 1, raise_at(half))
+    after(3, 1, 1, square_relu)
+
+    def start_lower():
+        for c in mate_blocks(mix_sem, precv1):
+            c.wait_send()
+        lower_at(0)()
+
+    after(3, 2, 0, start_lower)
+    for h in range(1, half - 1):
+        after(3, h + 1, 1, lower_at(h))
+    after(3, half, 0, lower_at(half - 1))
+    after(3, half, 0, lower_at(half))
+
+    for ti in range(4):
+        for e in events(ti):
+            event(*e)
+            for work in plan.get(e, ()):
+                work()
+
+    for c in mate_blocks(low_sem, precv2):
+        c.wait_recv()
+    norm(fst, precv2, norm2_ref, out_ref)
+
+    for c in mate_blocks(low_sem, precv2):
+        c.wait_send()
+    give.wait_send()
+    share.wait_send()
+    for key in copies:
+        copies[key].wait_send()
+
+
+def fits(mesh, args):
+    n = mesh.shape["fs"]
+    tokens, outer_weight = args[0], args[1]
+    d, wch = outer_weight.shape[0] * n, outer_weight.shape[1]
+    ff = args[7].shape[1]
+    rows = tokens.shape[0]
+    return (
+        mesh.shape["rep"] == 2
+        and mesh.shape["tp"] == 2
+        and n % 2 == 0
+        and n >= 8
+        and (d // n) % 128 == 0
+        and wch % 256 == 0
+        and ff % 256 == 0
+        and rows % SEQ == 0
+    )
+
+
+def fused(mesh, *args):
+    (
+        tokens,
+        outer_weight,
+        inner_weight,
+        value_weight,
+        conv_taps,
+        mix_out,
+        norm_first,
+        up_weight,
+        down_weight,
+        norm_second,
+    ) = args
+    n = mesh.shape["fs"]
+    rows, d = tokens.shape
+    ks, wch = outer_weight.shape
+    ff = up_weight.shape[1]
+    nc = mix_out.shape[1]
+    both = 2 * rows
+    anywhere = pl.BlockSpec(memory_space=pl.ANY)
+    vmem = pl.BlockSpec(memory_space=pltpu.VMEM)
+    messages = 4 * (3 * n - 3)
+    pairs = 2 + 2 * n
+    return pl.pallas_call(
+        functools.partial(layer_kernel, n),
+        out_shape=jax.ShapeDtypeStruct((rows, d), BF),
+        in_specs=[
+            anywhere,
+            anywhere,
+            anywhere,
+            anywhere,
+            vmem,
+            anywhere,
+            vmem,
+            anywhere,
+            anywhere,
+            vmem,
+        ],
+        out_specs=vmem,
+        scratch_shapes=[
+            pltpu.VMEM((3, n, ks, wch), BF),
+            pltpu.VMEM((n, wch, nc), BF),
+            pltpu.VMEM((n, ks, ff), BF),
+            pltpu.VMEM((n, ff, nc), BF),
+            pltpu.VMEM((3, ks, wch), F32),
+            pltpu.VMEM((wch, nc), F32),
+            pltpu.VMEM((ff, nc), F32),
+            pltpu.VMEM((both, d), BF),
+            pltpu.VMEM((both, max(3 * wch, ff)), F32),
+            pltpu.VMEM((both, wch), BF),
+            pltpu.VMEM((n, rows, nc), F32),
+            pltpu.VMEM((n, rows, nc), BF),
+            pltpu.VMEM((n, rows, nc), BF),
+            pltpu.VMEM((n, rows, nc), BF),
+            pltpu.VMEM((both, d), BF),
+            pltpu.VMEM((both, ff), BF),
+            pltpu.SemaphoreType.DMA((7,)),
+            pltpu.SemaphoreType.DMA((messages,)),
+            pltpu.SemaphoreType.DMA((messages,)),
+            pltpu.SemaphoreType.DMA((pairs,)),
+            pltpu.SemaphoreType.DMA((pairs,)),
+        ],
+        compiler_params=pltpu.CompilerParams(
+            collective_id=0, has_side_effects=True, vmem_limit_bytes=67043328
+        ),
+        name="layer",
+    )(
+        tokens,
+        outer_weight,
+        inner_weight,
+        value_weight,
+        conv_taps,
+        mix_out,
+        norm_first.reshape(1, d),
+        up_weight,
+        down_weight,
+        norm_second.reshape(1, d),
+    )
+
+
 def solution(mesh):
+    def body(*args):
+        return fused(mesh, *args) if fits(mesh, args) else local(*args)
+
     return jax.shard_map(
-        local,
+        body,
         mesh=mesh,
         in_specs=(
             P(("rep", "fs", "tp"), None),

time: 594 us -> 215 us (0.36)
  waiting for transfers between devices: 511 us -> 0 us
  Pallas kernels: 0 us -> 212 us
  matrix products: 46.1 us -> 0 us
  other arithmetic: 19.7 us -> 0 us
  between operations: 13.6 us -> 0.01 us
    all_gather x8 -> x0, waiting for transfers between devices: 495 us -> none  [the longest x1 120 us: local(): upward_full = lax.all_gather(upward_bf, 'fs', axis=0, tiled=True)]
    pallas_call x0 -> x1, Pallas kernels: none -> 212 us  [fused(): pl.pallas_call(functools.partial(layer_kernel, n), out_shape=jax.ShapeDty...]
    dot_general x5 -> x0, matrix products: 46.1 us -> none  [the longest x1 12.8 us: local(): jnp.dot(selected, mixout_full, preferred_element_type=jnp.float32)]
    reduce_scatter x2 -> x0, waiting for transfers between devices: 15.8 us -> none  [the longest x1 9.5 us: local(): lax.psum_scatter(jnp.dot(selected, down_full, preferred_element_type=jnp....]
    convert_element_type x8 -> x0, other arithmetic: 13.8 us -> none  [the longest x1 2.86 us: local(): upward_bf = up_weight.astype(jnp.bfloat16)]
  transfers between devices with their start and end apart: 10 -> 0, of which waited for: 10 -> 0; matrix products, arithmetic and copies ran while one was open for 7% -> 0% of each run, Pallas kernels for 0% -> 0%
where the time goes in v1:
time: 215 us
  Pallas kernels  212 us (99%)
  local copies, waits for them, and re-layouts  2.73 us (1%)
    pallas_call x1, Pallas kernels, fused(): pl.pallas_call(functools.partial(layer_kernel, n), out_shape=jax.ShapeDty...  212 us

profile of v1, /device:TPU:0, one launch (start us, length us, event | category | flops | bytes accessed | tf_op | source)
XLA Modules:
  0.0 214.7 jit_solution(8379663286325623548)
XLA Ops:
  0.0 212.0 %layer.1 = bf16[384,2048]{1,0:T(8,128)(2,1)} custom-call(bf16[384,2048]{1,0:T(8,128)(2,1)} %tokens_hbm.1, f32[256,768]{1,0:T(8,128)} %outer_hbm.1, f32[256,768]{1,0:T(8,128)} %inner_hbm.1, f32[256,768]{1,0:T(8,128)} %value_hbm.1, f32[3,768]{1,0:T(4,128)} %taps_ref.1, f32[768,256]{1,0:T(8,128)} %mix_hbm.1, f32[1,2048]{1,0:T(1,128)} %bitcast.2, ...), custom_call_target="tpu_custom_call" | custom-call | tf_op jit(solution)/shard_map/layer/pallas_call | solution.py:548
  212.0 2.7 %copy.12 = bf16[384,2048]{1,0:T(8,128)(2,1)} copy(bf16[384,2048]{1,0:T(8,128)(2,1)} %layer.1) | data formatting | bytes 3145728

commit v2 on v1

--- a/solution.py
+++ b/solution.py
@@ -115,9 +115,6 @@
     wb,
     wc,
     wd,
-    stage_a,
-    stage_b,
-    stage_d,
     tok,
     acc,
     mixed,
@@ -125,6 +122,8 @@
     psend,
     precv1,
     precv2,
+    xsend,
+    xrecv,
     fst,
     hid,
     load_sem,
@@ -132,6 +131,8 @@
     ring_recv,
     tp_send,
     tp_recv,
+    x_send,
+    x_recv,
 ):
     half = n // 2
     r = lax.axis_index("rep")
@@ -142,7 +143,7 @@
     d = tokens_hbm.shape[1]
     ks = wa.shape[2]
     wch = wa.shape[3]
-    ff = wc.shape[2]
+    ff = wc.shape[1]
     nc = wb.shape[2]
 
     odd = f % 2
@@ -158,17 +159,37 @@
     across = {"rep": 1 - r}
     mate = {"tp": 1 - t}
 
+    mine = pl.multiple_of(r * ff, 128)
+    first_down = min(ff, both)
+    rest_down = ff - first_down
     loads = [
-        pltpu.make_async_copy(outer_hbm, stage_a.at[0], load_sem.at[0]),
-        pltpu.make_async_copy(inner_hbm, stage_a.at[1], load_sem.at[1]),
-        pltpu.make_async_copy(value_hbm, stage_a.at[2], load_sem.at[2]),
-        pltpu.make_async_copy(mix_hbm, stage_b, load_sem.at[3]),
         pltpu.make_async_copy(
-            up_hbm, acc.at[pl.ds(0, ks), pl.ds(0, ff)], load_sem.at[4]
+            src, acc.at[pl.ds(i * ks, ks), pl.ds(0, wch)], load_sem.at[i]
+        )
+        for i, src in enumerate((outer_hbm, inner_hbm, value_hbm))
+    ]
+    loads += [
+        pltpu.make_async_copy(mix_hbm, own.at[0, pl.ds(0, wch)], load_sem.at[3]),
+        pltpu.make_async_copy(
+            up_hbm.at[:, pl.ds(mine, ff)],
+            acc.at[pl.ds(3 * ks, ks), pl.ds(0, ff)],
+            load_sem.at[4],
         ),
-        pltpu.make_async_copy(down_hbm, stage_d, load_sem.at[5]),
+        pltpu.make_async_copy(
+            down_hbm.at[pl.ds(mine, first_down)],
+            own.at[1, pl.ds(0, first_down)],
+            load_sem.at[5],
+        ),
         pltpu.make_async_copy(tokens_hbm, tok.at[pl.ds(0, rows)], load_sem.at[6]),
     ]
+    if rest_down:
+        loads.append(
+            pltpu.make_async_copy(
+                down_hbm.at[pl.ds(mine + first_down, rest_down)],
+                own.at[2, pl.ds(0, rest_down)],
+                load_sem.at[7],
+            )
+        )
     for load in loads:
         load.start()
 
@@ -187,14 +208,28 @@
             device_id_type=MESH,
         )
 
+    def across_copy(i, src, dst):
+        return pltpu.make_async_remote_copy(
+            src_ref=src,
+            dst_ref=dst,
+            send_sem=x_send.at[i],
+            recv_sem=x_recv.at[i],
+            device_id=across,
+            device_id_type=MESH,
+        )
+
     def piece(ti, which, owner):
         if ti == 0:
             return wa.at[2 if which else r, owner]
-        ref = (None, wb, wc, wd)[ti]
-        u = third_rows(ref.shape[1])
-        if which:
-            return ref.at[owner, pl.ds(2 * u, ref.shape[1] - 2 * u)]
-        return ref.at[owner, pl.ds(pl.multiple_of(r * u, 16), u)]
+        if ti == 1:
+            u = third_rows(wch)
+            if which:
+                return wb.at[owner, pl.ds(2 * u, wch - 2 * u)]
+            return wb.at[owner, pl.ds(pl.multiple_of(r * u, 16), u)]
+        if ti == 2:
+            u = ks // 2
+            return wc.at[pl.ds(pl.multiple_of(owner * ks + which * u, 16), u)]
+        return wd.at[owner, pl.ds(which * (ff // 2), ff // 2)]
 
     per = 6 * half - 3
     index = {}
@@ -209,7 +244,7 @@
     def message(ti, kind, h):
         key = (ti, kind, h)
         if key not in copies:
-            which = kind[1] == "p"
+            which = int(kind[1] == "p")
             if kind[0] == "R":
                 src, device = at(pos - (h - 1)), right
             elif kind[0] == "L":
@@ -229,7 +264,7 @@
         return copies[key]
 
     def send(ti, kind, h):
-        if ti < 4 and (kind, h) in index:
+        if ti < 4 and (kind, h) in index and (ti < 2 or kind[0] != "X"):
             message(ti, kind, h).start()
 
     def got(ti, kind, h):
@@ -282,7 +317,7 @@
 
     for i in range(3):
         loads[i].wait()
-        wa[i, f] = stage_a[i].astype(BF)
+        wa[i, f] = acc[pl.ds(i * ks, ks), pl.ds(0, wch)].astype(BF)
     send(0, "Rq", 1)
     send(0, "Lq", 1)
     send(0, "Rp", 1)
@@ -290,59 +325,126 @@
     share = mate_copy(0, tokens_hbm, tok.at[pl.ds(rows, rows)])
     share.start()
     loads[3].wait()
-    wb[f] = stage_b[...].astype(BF)
+    wb[f] = own[0, pl.ds(0, wch)].astype(BF)
     loads[4].wait()
-    wc[f] = acc[pl.ds(0, ks), pl.ds(0, ff)].astype(BF)
+    wc[pl.ds(pl.multiple_of(f * ks, 16), ks), :] = acc[
+        pl.ds(3 * ks, ks), pl.ds(0, ff)
+    ].astype(BF)
     loads[5].wait()
-    wd[f] = stage_d[...].astype(BF)
+    wd[f, pl.ds(0, first_down)] = own[1, pl.ds(0, first_down)].astype(BF)
+    if rest_down:
+        loads[7].wait()
+        wd[f, pl.ds(first_down, rest_down)] = own[2, pl.ds(0, rest_down)].astype(BF)
     loads[6].wait()
     share.wait_recv()
 
     tn = 256
-
-    def accumulate(x_ref, h, weight, width, base):
+    pieces = 2
+    pr = rows // pieces
+    mix_sem, first_sem = 1, 1 + n
+    diag_sem = first_sem + pieces
+    far_sem = diag_sem + pieces
+    near_sem = far_sem + n
+    OWN, TWIN, MATE, DIAG = 0, rows, 2 * rows, 3 * rows
+
+    def accumulate(x_ref, gap, h, weight, width, dest):
         who = owners(h)
 
         def unit(i, _):
-            m = pl.multiple_of((i % 2) * rows, 16)
-            c = pl.multiple_of((i // 2) * tn, tn)
+            side = i % 2
+            c = i // 2
             total = None
             for o in who:
-                x = x_ref[pl.ds(m, rows), pl.ds(pl.multiple_of(o * ks, 128), ks)]
-                term = dot(x, weight(o, pl.ds(c, tn)))
+                x = x_ref[
+                    pl.ds(pl.multiple_of(side * gap, 16), rows),
+                    pl.ds(pl.multiple_of(o * ks, 128), ks),
+                ]
+                term = dot(x, weight(o, pl.ds(pl.multiple_of(c * tn, tn), tn)))
                 total = term if total is None else total + term
-            span = pl.ds(pl.multiple_of(base + c, tn), tn)
+            view = dest(pl.multiple_of(side * rows, 16), c)
             if h == 0:
-                acc[pl.ds(m, rows), span] = total
+                view[...] = total
             else:
-                acc[pl.ds(m, rows), span] += total
+                view[...] += total
             return 0
 
         lax.fori_loop(0, 2 * (width // tn), unit, 0)
+
+    def acc_at(base):
+        def dest(m, c):
+            return acc.at[
+                pl.ds(base + m, rows), pl.ds(pl.multiple_of(c * tn, tn), tn)
+            ]
+
+        return dest
 
     def project(h):
         for i in range(3):
-            accumulate(tok, h, lambda o, c, i=i: wa[i, o, :, c], wch, i * wch)
-
-    def raise_(h):
-        accumulate(fst, h, lambda o, c: wc[o, :, c], ff, 0)
-
-    def lower(x_ref, w_ref, h, recv, first_sem):
-        for k, o in enumerate(owners(h)):
-            psend[o] = dot(x_ref[pl.ds(rows, rows), :], w_ref[o]).astype(BF)
-            mate_block(first_sem, h, k, o, recv).start()
-            own[o] = dot(x_ref[pl.ds(0, rows), :], w_ref[o])
-
-    def mate_block(first_sem, h, k, o, recv):
-        i = first_sem + (0 if h == 0 else 2 * h - 1 + k)
-        return mate_copy(i, psend.at[o], recv.at[o])
-
-    def mate_blocks(first_sem, recv):
-        return [
-            mate_block(first_sem, h, k, o, recv)
-            for h in range(half + 1)
-            for k, o in enumerate(owners(h))
-        ]
+            dest = (
+                acc_at(i * both)
+                if i < 2
+                else lambda m, c: own.at[c, pl.ds(m, rows), :]
+            )
+            accumulate(tok, rows, h, lambda o, c, i=i: wa[i, o, :, c], wch, dest)
+
+    def raise_near(h):
+        def weight(o, c):
+            return wc[pl.ds(pl.multiple_of(o * ks, 16), ks), c]
+
+        accumulate(fst, MATE, h, weight, ff, acc_at(0))
+
+    def raise_far(start):
+        def unit(i, _):
+            c = pl.ds(pl.multiple_of(i * tn, tn), tn)
+            v = jnp.maximum(dot(fst[pl.ds(start, pr), :], wc[:, c]), 0.0)
+            hid[pl.ds(start, pr), c] = (v * v).astype(BF)
+            return 0
+
+        lax.fori_loop(0, ff // tn, unit, 0)
+
+    def numbered(h):
+        return [(0 if h == 0 else 2 * h - 1 + k, o) for k, o in enumerate(owners(h))]
+
+    every = [item for h in range(half + 1) for item in numbered(h)]
+
+    def mix_block(k, o):
+        return mate_copy(mix_sem + k, psend.at[o, pl.ds(0, rows)], precv1.at[o])
+
+    def near_block(k, o):
+        part = pl.ds(0, rows)
+        return mate_copy(near_sem + k, psend.at[o, part], precv2.at[o, part])
+
+    def far_block(k, o):
+        part = pl.ds(rows, rows)
+        return mate_copy(far_sem + k, psend.at[o, part], precv2.at[o, part])
+
+    def across_block(k, o):
+        return across_copy(pieces + k, xsend.at[o], xrecv.at[o])
+
+    def mixout(h):
+        for k, o in numbered(h):
+            psend[o, pl.ds(0, rows)] = dot(mixed[pl.ds(rows, rows), :], wb[o]).astype(BF)
+            mix_block(k, o).start()
+            own[o, pl.ds(0, rows)] = dot(mixed[pl.ds(0, rows), :], wb[o])
+
+    def lower_far(h):
+        for k, o in numbered(h):
+            psend[o, pl.ds(rows, rows)] = dot(hid[pl.ds(DIAG, rows), :], wd[o]).astype(BF)
+            far_block(k, o).start()
+            own[o, pl.ds(rows, rows)] = dot(hid[pl.ds(TWIN, rows), :], wd[o])
+
+    def pass_across(h):
+        for k, o in numbered(h):
+            far_block(k, o).wait_recv()
+            part = pl.ds(rows, rows)
+            xsend[o] = (own[o, part] + precv2[o, part].astype(F32)).astype(BF)
+            across_block(k, o).start()
+
+    def lower_near(h):
+        for k, o in numbered(h):
+            psend[o, pl.ds(0, rows)] = dot(hid[pl.ds(MATE, rows), :], wd[o]).astype(BF)
+            near_block(k, o).start()
+            own[o, pl.ds(0, rows)] = dot(hid[pl.ds(OWN, rows), :], wd[o])
 
     def mix():
         seq = SEQ
@@ -352,8 +454,8 @@
             c = pl.multiple_of((i // (both // seq)) * tn, tn)
             o = acc[pl.ds(m, seq), pl.ds(c, tn)]
             p = (
-                acc[pl.ds(m, seq), pl.ds(pl.multiple_of(wch + c, tn), tn)]
-                * acc[pl.ds(m, seq), pl.ds(pl.multiple_of(2 * wch + c, tn), tn)]
+                acc[pl.ds(both + m, seq), pl.ds(c, tn)]
+                * own[i // (both // seq), pl.ds(m, seq), :]
             )
             place = lax.broadcasted_iota(jnp.int32, p.shape, 0)
             before = jnp.where(place > 0, pltpu.roll(p, 1, 0), 0.0)
@@ -365,18 +467,21 @@
 
         lax.fori_loop(0, (both // seq) * (wch // tn), unit, 0)
 
-    def norm(base_ref, recv, gain_ref, dest_ref):
+    def norm(base_ref, terms, gain_ref, dest_ref, start, count):
         tm = 32
 
         def unit(i, _):
-            m = pl.multiple_of(i * tm, tm)
-            parts = [
-                residual_scale
-                * base_ref[pl.ds(m, tm), pl.ds(b * nc, nc)].astype(F32)
-                + own[b, pl.ds(m, tm)]
-                + recv[b, pl.ds(m, tm)].astype(F32)
-                for b in range(n)
-            ]
+            m = pl.multiple_of(start + i * tm, tm)
+            parts = []
+            for b in range(n):
+                part = (
+                    residual_scale
+                    * base_ref[pl.ds(m, tm), pl.ds(b * nc, nc)].astype(F32)
+                    + own[b, pl.ds(m, tm)]
+                )
+                for term in terms:
+                    part = part + term[b, pl.ds(m, tm)].astype(F32)
+                parts.append(part)
             total = parts[0]
             for b in range(1, n):
                 total = total + parts[b]
@@ -394,25 +499,66 @@
                 ).astype(BF)
             return 0
 
-        lax.fori_loop(0, rows // tm, unit, 0)
-
-    def square_relu():
+        lax.fori_loop(0, count // tm, unit, 0)
+
+    def square_near():
         def unit(i, _):
-            m = pl.multiple_of((i % (both // 128)) * 128, 128)
-            c = pl.multiple_of((i // (both // 128)) * tn, tn)
-            v = jnp.maximum(acc[pl.ds(m, 128), pl.ds(c, tn)], 0.0)
-            hid[pl.ds(m, 128), pl.ds(c, tn)] = (v * v).astype(BF)
+            tiles = rows // 128
+            side = i % 2
+            m = pl.multiple_of(((i // 2) % tiles) * 128, 128)
+            c = pl.ds(pl.multiple_of((i // (2 * tiles)) * tn, tn), tn)
+            v = jnp.maximum(acc[pl.ds(side * rows + m, 128), c], 0.0)
+            hid[pl.ds(side * MATE + m, 128), c] = (v * v).astype(BF)
             return 0
 
-        lax.fori_loop(0, (both // 128) * (ff // tn), unit, 0)
-
-    mix_sem, first_sem, low_sem = 1, 1 + n, 2 + n
-    give = mate_copy(first_sem, fst.at[pl.ds(0, rows)], fst.at[pl.ds(rows, rows)])
+        lax.fori_loop(0, 2 * (rows // 128) * (ff // tn), unit, 0)
+
+    def near_first(p):
+        return mate_copy(
+            first_sem + p, fst.at[pl.ds(p * pr, pr)], fst.at[pl.ds(MATE + p * pr, pr)]
+        )
+
+    def twin_first(p):
+        return across_copy(
+            p, fst.at[pl.ds(p * pr, pr)], fst.at[pl.ds(TWIN + p * pr, pr)]
+        )
+
+    def diag_first(p):
+        return mate_copy(
+            diag_sem + p,
+            fst.at[pl.ds(TWIN + p * pr, pr)],
+            fst.at[pl.ds(DIAG + p * pr, pr)],
+        )
+
+    def make_first():
+        for k, o in every:
+            mix_block(k, o).wait_recv()
+        for p in range(pieces):
+            norm(tok, (precv1,), norm1_ref, fst, p * pr, pr)
+            twin_first(p).start()
+            near_first(p).start()
+
+    def take_near():
+        for p in range(pieces):
+            near_first(p).wait_recv()
+
+    def relay_first(p):
+        twin_first(p).wait_recv()
+        diag_first(p).start()
+
+    def far(p):
+        raise_far(TWIN + p * pr)
+        diag_first(p).wait_recv()
+        raise_far(DIAG + p * pr)
+
+    def free_sends():
+        for k, o in every:
+            mix_block(k, o).wait_send()
 
     plan = {}
 
-    def after(ti, h, which, work):
-        plan.setdefault((ti, h, which), []).append(work)
+    def after(ti, h, which, *work):
+        plan.setdefault((ti, h, which), []).extend(work)
 
     def project_at(h):
         def work():
@@ -426,65 +572,39 @@
         def work():
             if h:
                 arrived(1, h)
-            lower(mixed, wb, h, precv1, mix_sem)
+            mixout(h)
 
         return work
 
-    def raise_at(h):
-        def work():
-            if h:
-                arrived(2, h)
-            raise_(h)
-
-        return work
-
-    def lower_at(h):
-        def work():
-            if h:
-                arrived(3, h)
-            lower(hid, wd, h, precv2, low_sem)
-
-        return work
-
-    def first_half():
-        for c in mate_blocks(mix_sem, precv1):
-            c.wait_recv()
-        norm(tok, precv1, norm1_ref, fst)
-        give.start()
-
-    def start_raise():
-        give.wait_recv()
-        raise_(0)
-
-    after(0, 1, 0, lambda: project(0))
-    for h in range(1, half - 1):
+    def do(function, *values):
+        return lambda: function(*values)
+
+    last = half - 1
+    after(0, 1, 0, project_at(0))
+    for h in range(1, last):
         after(0, h + 1, 1, project_at(h))
-    after(1, 1, 0, project_at(half - 1))
+    after(1, 1, 0, project_at(last))
     after(1, 1, 1, project_at(half))
     after(1, 2, 0, mix)
-    after(1, half - 1, 0, mixout_at(0))
-    for h in range(1, half - 1):
-        after(1, half - 1 if h < half - 2 else half, 0, mixout_at(h))
-    after(2, 1, 0, mixout_at(half - 1))
-    after(2, 1, 0, mixout_at(half))
-    after(2, 1, 1, first_half)
-    after(2, 2, 0, start_raise)
-    for h in range(1, half - 1):
-        after(2, h + 1, 1, raise_at(h))
-    after(3, 1, 0, raise_at(half - 1))
-    after(3, 1, 1, raise_at(half))
-    after(3, 1, 1, square_relu)
-
-    def start_lower():
-        for c in mate_blocks(mix_sem, precv1):
-            c.wait_send()
-        lower_at(0)()
-
-    after(3, 2, 0, start_lower)
-    for h in range(1, half - 1):
-        after(3, h + 1, 1, lower_at(h))
-    after(3, half, 0, lower_at(half - 1))
-    after(3, half, 0, lower_at(half))
+    after(1, last, 0, mixout_at(0))
+    for h in range(1, half + 1):
+        after(1, last if h < last - 1 else half, 0, mixout_at(h))
+    after(1, half, 0, make_first)
+    after(2, 1, 0, take_near, do(raise_near, 0))
+    for h in range(1, last):
+        after(2, h + 1, 1, do(raise_near, h))
+    after(2, last, 0, do(relay_first, 0))
+    after(2, half, 0, do(raise_near, last), do(raise_near, half), do(far, 0))
+    for p in range(1, pieces):
+        after(3, 1, 0, do(relay_first, p), do(far, p))
+    after(3, 1, 1, free_sends, do(lower_far, 0), do(lower_far, 1))
+    after(3, 1, 1, do(pass_across, 0))
+    after(3, 2, 0, do(pass_across, 1), square_near)
+    for h in range(2, half):
+        after(3, h, 1, do(lower_far, h), do(lower_near, h - 2), do(pass_across, h))
+    after(3, half, 0, do(lower_far, half), do(lower_near, half - 2))
+    after(3, half, 0, do(pass_across, half))
+    after(3, half, 0, do(lower_near, half - 1), do(lower_near, half))
 
     for ti in range(4):
         for e in events(ti):
@@ -492,13 +612,20 @@
             for work in plan.get(e, ()):
                 work()
 
-    for c in mate_blocks(low_sem, precv2):
-        c.wait_recv()
-    norm(fst, precv2, norm2_ref, out_ref)
-
-    for c in mate_blocks(low_sem, precv2):
-        c.wait_send()
-    give.wait_send()
+    for k, o in every:
+        near_block(k, o).wait_recv()
+    for k, o in every:
+        across_block(k, o).wait_recv()
+    norm(fst, (precv2, xrecv), norm2_ref, out_ref, 0, rows)
+
+    for k, o in every:
+        near_block(k, o).wait_send()
+        far_block(k, o).wait_send()
+        across_block(k, o).wait_send()
+    for p in range(pieces):
+        near_first(p).wait_send()
+        twin_first(p).wait_send()
+        diag_first(p).wait_send()
     share.wait_send()
     for key in copies:
         copies[key].wait_send()
@@ -506,18 +633,23 @@
 
 def fits(mesh, args):
     n = mesh.shape["fs"]
-    tokens, outer_weight = args[0], args[1]
-    d, wch = outer_weight.shape[0] * n, outer_weight.shape[1]
-    ff = args[7].shape[1]
-    rows = tokens.shape[0]
+    rows, d = args[0].shape
+    ks, wch = args[1].shape
+    nc = args[5].shape[1]
+    ff = args[7].shape[1] // 2
     return (
         mesh.shape["rep"] == 2
         and mesh.shape["tp"] == 2
         and n % 2 == 0
         and n >= 8
-        and (d // n) % 128 == 0
+        and ks % 128 == 0
+        and nc == 256
         and wch % 256 == 0
         and ff % 256 == 0
+        and wch // 256 <= n
+        and wch <= 2 * rows
+        and ff <= 4 * rows
+        and ks <= rows
         and rows % SEQ == 0
     )
 
@@ -538,13 +670,13 @@
     n = mesh.shape["fs"]
     rows, d = tokens.shape
     ks, wch = outer_weight.shape
-    ff = up_weight.shape[1]
+    ff = up_weight.shape[1] // 2
     nc = mix_out.shape[1]
     both = 2 * rows
     anywhere = pl.BlockSpec(memory_space=pl.ANY)
     vmem = pl.BlockSpec(memory_space=pltpu.VMEM)
     messages = 4 * (3 * n - 3)
-    pairs = 2 + 2 * n
+    pairs = 5 + 3 * n
     return pl.pallas_call(
         functools.partial(layer_kernel, n),
         out_shape=jax.ShapeDtypeStruct((rows, d), BF),
@@ -564,25 +696,26 @@
         scratch_shapes=[
             pltpu.VMEM((3, n, ks, wch), BF),
             pltpu.VMEM((n, wch, nc), BF),
-            pltpu.VMEM((n, ks, ff), BF),
+            pltpu.VMEM((n * ks, ff), BF),
             pltpu.VMEM((n, ff, nc), BF),
-            pltpu.VMEM((3, ks, wch), F32),
-            pltpu.VMEM((wch, nc), F32),
-            pltpu.VMEM((ff, nc), F32),
             pltpu.VMEM((both, d), BF),
-            pltpu.VMEM((both, max(3 * wch, ff)), F32),
+            pltpu.VMEM((2 * both, max(wch, ff)), F32),
             pltpu.VMEM((both, wch), BF),
-            pltpu.VMEM((n, rows, nc), F32),
+            pltpu.VMEM((n, both, nc), F32),
+            pltpu.VMEM((n, both, nc), BF),
+            pltpu.VMEM((n, rows, nc), BF),
+            pltpu.VMEM((n, both, nc), BF),
             pltpu.VMEM((n, rows, nc), BF),
             pltpu.VMEM((n, rows, nc), BF),
-            pltpu.VMEM((n, rows, nc), BF),
-            pltpu.VMEM((both, d), BF),
-            pltpu.VMEM((both, ff), BF),
-            pltpu.SemaphoreType.DMA((7,)),
+            pltpu.VMEM((2 * both, d), BF),
+            pltpu.VMEM((2 * both, ff), BF),
+            pltpu.SemaphoreType.DMA((8,)),
             pltpu.SemaphoreType.DMA((messages,)),
             pltpu.SemaphoreType.DMA((messages,)),
             pltpu.SemaphoreType.DMA((pairs,)),
             pltpu.SemaphoreType.DMA((pairs,)),
+            pltpu.SemaphoreType.DMA((2 + n,)),
+            pltpu.SemaphoreType.DMA((2 + n,)),
         ],
         compiler_params=pltpu.CompilerParams(
             collective_id=0, has_side_effects=True, vmem_limit_bytes=67043328

time: 215 us -> 199 us (0.926)
  Pallas kernels: 212 us -> 196 us
    pallas_call x1, Pallas kernels: 212 us -> 196 us  [fused(): pl.pallas_call(functools.partial(layer_kernel, n), out_shape=jax.ShapeDty...]
where the time goes in v2:
time: 199 us; the launch traced here: 198 us
  Pallas kernels  196 us (98%)
  local copies, waits for them, and re-layouts  2.73 us (1%)
    pallas_call x1, Pallas kernels, fused(): pl.pallas_call(functools.partial(layer_kernel, n), out_shape=jax.ShapeDty...  196 us

profile of v2, /device:TPU:0, one launch (start us, length us, event | category | flops | bytes accessed | tf_op | source)
XLA Modules:
  0.0 198.3 jit_solution(6267113913894797130)
XLA Ops:
  0.0 195.6 %layer.1 = bf16[384,2048]{1,0:T(8,128)(2,1)} custom-call(bf16[384,2048]{1,0:T(8,128)(2,1)} %tokens_hbm.1, f32[256,768]{1,0:T(8,128)} %outer_hbm.1, f32[256,768]{1,0:T(8,128)} %inner_hbm.1, f32[256,768]{1,0:T(8,128)} %value_hbm.1, f32[3,768]{1,0:T(4,128)} %taps_ref.1, f32[768,256]{1,0:T(8,128)} %mix_hbm.1, f32[1,2048]{1,0:T(1,128)} %bitcast.2, ...), custom_call_target="tpu_custom_call" | custom-call | tf_op jit(solution)/shard_map/layer/pallas_call | solution.py:680
  195.6 2.7 %copy.12 = bf16[384,2048]{1,0:T(8,128)(2,1)} copy(bf16[384,2048]{1,0:T(8,128)(2,1)} %layer.1) | data formatting | bytes 3145728

commit v3 on v2

--- a/solution.py
+++ b/solution.py
@@ -94,10 +94,6 @@
     return jnp.dot(a, b, preferred_element_type=F32)
 
 
-def third_rows(rows):
-    return (rows // 3 + 8) // 16 * 16
-
-
 def layer_kernel(
     n,
     tokens_hbm,
@@ -190,7 +186,7 @@
                 load_sem.at[7],
             )
         )
-    for load in loads:
+    for load in loads[:3]:
         load.start()
 
     barrier = pltpu.get_barrier_semaphore()
@@ -222,7 +218,7 @@
         if ti == 0:
             return wa.at[2 if which else r, owner]
         if ti == 1:
-            u = third_rows(wch)
+            u = wch // 64 * 16
             if which:
                 return wb.at[owner, pl.ds(2 * u, wch - 2 * u)]
             return wb.at[owner, pl.ds(pl.multiple_of(r * u, 16), u)]
@@ -275,25 +271,24 @@
             got(ti, "Rq", h)
             send(ti, "Rq", h + 1)
             send(ti, "XR", h)
-            if h < half:
-                got(ti, "Lq", h)
-                if h + 1 < half:
-                    send(ti, "Lq", h + 1)
-                else:
-                    send(ti + 1, "Lq", 1)
-                send(ti, "XL", h)
-            else:
+            if h == half:
                 send(ti + 1, "Rp", 1)
-                got(ti, "Lp", h)
-                send(ti + 1, "Lp", 1)
+            got(ti, "Lp", h)
+            send(ti, "Lp", h + 1)
+            if h == half:
+                send(ti + 1, "Lq", 1)
         else:
             got(ti, "Rp", h)
             if h + 1 < half:
                 send(ti, "Rp", h + 1)
             else:
                 send(ti + 1, "Rq", 1)
-            got(ti, "Lp", h)
-            send(ti, "Lp", h + 1)
+            got(ti, "Lq", h)
+            if h + 1 < half:
+                send(ti, "Lq", h + 1)
+            else:
+                send(ti + 1, "Lp", 1)
+            send(ti, "XL", h)
 
     def events(ti):
         out = []
@@ -319,9 +314,11 @@
         loads[i].wait()
         wa[i, f] = acc[pl.ds(i * ks, ks), pl.ds(0, wch)].astype(BF)
     send(0, "Rq", 1)
+    send(0, "Lp", 1)
+    send(0, "Rp", 1)
     send(0, "Lq", 1)
-    send(0, "Rp", 1)
-    send(0, "Lp", 1)
+    for load in loads[3:]:
+        load.start()
     share = mate_copy(0, tokens_hbm, tok.at[pl.ds(rows, rows)])
     share.start()
     loads[3].wait()
@@ -339,7 +336,7 @@
     share.wait_recv()
 
     tn = 256
-    pieces = 2
+    pieces = 4
     pr = rows // pieces
     mix_sem, first_sem = 1, 1 + n
     diag_sem = first_sem + pieces
@@ -378,8 +375,8 @@
 
         return dest
 
-    def project(h):
-        for i in range(3):
+    def project(h, tensors=(0, 1, 2)):
+        for i in tensors:
             dest = (
                 acc_at(i * both)
                 if i < 2
@@ -387,20 +384,38 @@
             )
             accumulate(tok, rows, h, lambda o, c, i=i: wa[i, o, :, c], wch, dest)
 
+    def raise_part(size, start, x_base, acc_base, hs, new, final):
+        who = [o for h in hs for o in owners(h)]
+        tiles = ff // tn
+
+        def unit(i, _):
+            side = i % 2
+            c = pl.ds(pl.multiple_of(i // 2 * tn, tn), tn)
+            x_row = pl.multiple_of(x_base + side * MATE + start, 16)
+            total = None
+            for o in who:
+                x = fst[
+                    pl.ds(x_row, size), pl.ds(pl.multiple_of(o * ks, 128), ks)
+                ]
+                term = dot(x, wc[pl.ds(pl.multiple_of(o * ks, 16), ks), c])
+                total = term if total is None else total + term
+            span = pl.ds(pl.multiple_of(acc_base + side * rows + start, 16), size)
+            if not new:
+                total = total + acc[span, c]
+            if final:
+                total = jnp.maximum(total, 0.0)
+                hid[pl.ds(x_row, size), c] = (total * total).astype(BF)
+            else:
+                acc[span, c] = total
+            return 0
+
+        lax.fori_loop(0, 2 * tiles, unit, 0)
+
     def raise_near(h):
-        def weight(o, c):
-            return wc[pl.ds(pl.multiple_of(o * ks, 16), ks), c]
-
-        accumulate(fst, MATE, h, weight, ff, acc_at(0))
-
-    def raise_far(start):
-        def unit(i, _):
-            c = pl.ds(pl.multiple_of(i * tn, tn), tn)
-            v = jnp.maximum(dot(fst[pl.ds(start, pr), :], wc[:, c]), 0.0)
-            hid[pl.ds(start, pr), c] = (v * v).astype(BF)
-            return 0
-
-        lax.fori_loop(0, ff // tn, unit, 0)
+        raise_part(rows, 0, OWN, 0, [h], h == 0, h == half)
+
+    def raise_far(p, count, hs):
+        raise_part(pr * count, p * pr, TWIN, both, hs, 0 in hs, half in hs)
 
     def numbered(h):
         return [(0 if h == 0 else 2 * h - 1 + k, o) for k, o in enumerate(owners(h))]
@@ -501,18 +516,6 @@
 
         lax.fori_loop(0, count // tm, unit, 0)
 
-    def square_near():
-        def unit(i, _):
-            tiles = rows // 128
-            side = i % 2
-            m = pl.multiple_of(((i // 2) % tiles) * 128, 128)
-            c = pl.ds(pl.multiple_of((i // (2 * tiles)) * tn, tn), tn)
-            v = jnp.maximum(acc[pl.ds(side * rows + m, 128), c], 0.0)
-            hid[pl.ds(side * MATE + m, 128), c] = (v * v).astype(BF)
-            return 0
-
-        lax.fori_loop(0, 2 * (rows // 128) * (ff // tn), unit, 0)
-
     def near_first(p):
         return mate_copy(
             first_sem + p, fst.at[pl.ds(p * pr, pr)], fst.at[pl.ds(MATE + p * pr, pr)]
@@ -546,10 +549,9 @@
         twin_first(p).wait_recv()
         diag_first(p).start()
 
-    def far(p):
-        raise_far(TWIN + p * pr)
-        diag_first(p).wait_recv()
-        raise_far(DIAG + p * pr)
+    def take_far(p, count):
+        for q in range(p, p + count):
+            diag_first(q).wait_recv()
 
     def free_sends():
         for k, o in every:
@@ -580,31 +582,36 @@
         return lambda: function(*values)
 
     last = half - 1
+    until = list(range(half))
+    most = pieces - 1
     after(0, 1, 0, project_at(0))
     for h in range(1, last):
         after(0, h + 1, 1, project_at(h))
-    after(1, 1, 0, project_at(last))
-    after(1, 1, 1, project_at(half))
-    after(1, 2, 0, mix)
-    after(1, last, 0, mixout_at(0))
-    for h in range(1, half + 1):
-        after(1, last if h < last - 1 else half, 0, mixout_at(h))
+    after(1, 1, 0, do(arrived, 0, last), do(project, last, (0,)))
+    after(1, 1, 1, do(project, last, (1,)))
+    after(1, 2, 0, do(project, last, (2,)))
+    after(1, 2, 1, project_at(half))
+    after(1, last, 0, mix)
+    for h in range(half + 1):
+        after(1, *((last, 1) if h < last - 1 else (half, 0)), mixout_at(h))
     after(1, half, 0, make_first)
     after(2, 1, 0, take_near, do(raise_near, 0))
-    for h in range(1, last):
-        after(2, h + 1, 1, do(raise_near, h))
-    after(2, last, 0, do(relay_first, 0))
-    after(2, half, 0, do(raise_near, last), do(raise_near, half), do(far, 0))
-    for p in range(1, pieces):
-        after(3, 1, 0, do(relay_first, p), do(far, p))
-    after(3, 1, 1, free_sends, do(lower_far, 0), do(lower_far, 1))
-    after(3, 1, 1, do(pass_across, 0))
-    after(3, 2, 0, do(pass_across, 1), square_near)
-    for h in range(2, half):
-        after(3, h, 1, do(lower_far, h), do(lower_near, h - 2), do(pass_across, h))
-    after(3, half, 0, do(lower_far, half), do(lower_near, half - 2))
-    after(3, half, 0, do(pass_across, half))
-    after(3, half, 0, do(lower_near, half - 1), do(lower_near, half))
+    for h in range(1, half):
+        after(2, h, 1, do(raise_near, h))
+    after(2, 2, 0, do(relay_first, 0))
+    after(2, 2, 1, do(relay_first, 1))
+    for p in range(2, most):
+        after(2, last, 1, do(relay_first, p))
+    after(2, last, 1, do(take_far, 0, most), do(raise_far, 0, most, until))
+    after(2, half, 0, do(relay_first, most))
+    after(2, half, 0, do(raise_far, 0, most, [half]), do(take_far, most, 1))
+    after(2, half, 0, do(raise_far, most, 1, until + [half]))
+    after(2, half, 0, do(lower_far, 0), do(raise_near, half), do(pass_across, 0))
+    after(3, 1, 0, free_sends)
+    for h in range(1, half):
+        after(3, h, 1, do(lower_far, h), do(lower_near, h - 1), do(pass_across, h))
+    after(3, half, 0, do(lower_far, half), do(lower_near, half - 1))
+    after(3, half, 0, do(pass_across, half), do(lower_near, half))
 
     for ti in range(4):
         for e in events(ti):
@@ -651,6 +658,7 @@
         and ff <= 4 * rows
         and ks <= rows
         and rows % SEQ == 0
+        and rows % 128 == 0
     )
 
 
@@ -676,7 +684,7 @@
     anywhere = pl.BlockSpec(memory_space=pl.ANY)
     vmem = pl.BlockSpec(memory_space=pltpu.VMEM)
     messages = 4 * (3 * n - 3)
-    pairs = 5 + 3 * n
+    pairs = 9 + 3 * n
     return pl.pallas_call(
         functools.partial(layer_kernel, n),
         out_shape=jax.ShapeDtypeStruct((rows, d), BF),
@@ -714,8 +722,8 @@
             pltpu.SemaphoreType.DMA((messages,)),
             pltpu.SemaphoreType.DMA((pairs,)),
             pltpu.SemaphoreType.DMA((pairs,)),
-            pltpu.SemaphoreType.DMA((2 + n,)),
-            pltpu.SemaphoreType.DMA((2 + n,)),
+            pltpu.SemaphoreType.DMA((4 + n,)),
+            pltpu.SemaphoreType.DMA((4 + n,)),
         ],
         compiler_params=pltpu.CompilerParams(
             collective_id=0, has_side_effects=True, vmem_limit_bytes=67043328

time: 199 us -> 191 us (0.960)
  Pallas kernels: 196 us -> 188 us
    pallas_call x1, Pallas kernels: 196 us -> 188 us  [fused(): pl.pallas_call(functools.partial(layer_kernel, n), out_shape=jax.ShapeDty...]
where the time goes in v3:
time: 191 us; the launch traced here: 190 us
  Pallas kernels  188 us (98%)
  local copies, waits for them, and re-layouts  2.73 us (1%)
    pallas_call x1, Pallas kernels, fused(): pl.pallas_call(functools.partial(layer_kernel, n), out_shape=jax.ShapeDty...  188 us

profile of v3, /device:TPU:0, one launch (start us, length us, event | category | flops | bytes accessed | tf_op | source)
XLA Modules:
  0.0 190.3 jit_solution(3297199018411436793)
XLA Ops:
  0.0 187.6 %layer.1 = bf16[384,2048]{1,0:T(8,128)(2,1)} custom-call(bf16[384,2048]{1,0:T(8,128)(2,1)} %tokens_hbm.1, f32[256,768]{1,0:T(8,128)} %outer_hbm.1, f32[256,768]{1,0:T(8,128)} %inner_hbm.1, f32[256,768]{1,0:T(8,128)} %value_hbm.1, f32[3,768]{1,0:T(4,128)} %taps_ref.1, f32[768,256]{1,0:T(8,128)} %mix_hbm.1, f32[1,2048]{1,0:T(1,128)} %bitcast.2, ...), custom_call_target="tpu_custom_call" | custom-call | tf_op jit(solution)/shard_map/layer/pallas_call | solution.py:688
  187.6 2.7 %copy.12 = bf16[384,2048]{1,0:T(8,128)(2,1)} copy(bf16[384,2048]{1,0:T(8,128)(2,1)} %layer.1) | data formatting | bytes 3145728
